TPU v7x, 32 devices: a whole 2x2x4 slice. The times are simulated.
32 devices in a mesh: sp: 4 (over z), tp: 8 (over y, x, core).
Axes of the slice: x: 2, y: 2, z: 4, core: 2. Of those that a mesh axis runs over, the one named last changes fastest.
Arguments:
- target: bfloat16 [512, 2048], P('sp'), may hold values from -6 to 6
- source: bfloat16 [1024, 2048], P(('sp', 'tp')), may hold values from -6 to 6
- cotangent: bfloat16 [512, 2048], P('sp'), may hold values from -6 to 6
- target_gain: float32 [2048], replicated, may hold values from 0.1 to 1.9
- source_gain: float32 [2048], replicated, may hold values from 0.1 to 1.9
- query_weight: bfloat16 [2048, 8192], P(None, 'tp'), may hold values from -4 to 4
- key_weight: bfloat16 [2048, 2048], P(None, 'tp'), may hold values from -1 to 1
- value_projection_weight: bfloat16 [2048, 2048], P(None, 'tp'), may hold values from -0.125 to 0.125
- output_weight: bfloat16 [8192, 2048], P('tp'), may hold values from -0.0625 to 0.0625
Outputs:
- target_grad: float32 [512, 2048], P(('sp', 'tp'))
- source_grad: float32 [1024, 2048], P(('sp', 'tp'))
- key_weight_grad: float32 [2048, 2048], P(None, 'tp')
All inputs are finite; a program needn't handle non-finite values.
Results may differ from a plain program's by a relative error of at most 0.018.
The roundings to bfloat16 on the way count: a program that leaves them out, or rounds other values in their place, can miss the bound.
Values may be sent and summed in bfloat16 or wider, within the bound.
A program may use at most 64 MiB of HBM per device.

v0:
```python
import jax
import jax.numpy as jnp
from jax import lax
from jax.sharding import PartitionSpec as P

HEAD_SIZE = 256
EPSILON = 1e-05


def as_sent(array):

    def short(part):
        return part.astype(jnp.bfloat16) if part.dtype == jnp.float32 else part

    return jax.tree.map(short, array)


def partner_2(value, axis, bit):
    mask = 2**bit
    pairs = [(source, source ^ mask) for source in range(lax.axis_size(axis))]
    return lax.ppermute(value, axis, pairs)


def combined_all(value, axis, join):
    pieces = jax.tree.map(lambda part: lax.all_gather(part, axis), value)
    head = jax.tree.map(lambda part: part[0], pieces)
    tail = jax.tree.map(lambda part: part[1:], pieces)
    running, _ = lax.scan(lambda running, piece: (join(running, piece), None), head, tail)
    return running


def norm_rows(rows):
    values = rows.astype(jnp.float32)
    centred = values - jnp.mean(values, axis=-1, keepdims=True)
    inverse = lax.rsqrt(jnp.mean(centred * centred, axis=-1, keepdims=True) + EPSILON)
    return (centred * inverse, inverse)


def norm_back(scaled, inverse, gain, upstream):
    weighted = upstream * gain
    spread = jnp.mean(weighted * scaled, axis=-1, keepdims=True)
    return inverse * (weighted - jnp.mean(weighted, axis=-1, keepdims=True) - scaled * spread)


def times_transposed(left, right):
    return lax.dot_general(
        left, right, (((1,), (1,)), ((), ())), preferred_element_type=jnp.float32
    )


def split_heads(flat):
    return flat.reshape(flat.shape[0], flat.shape[1] // HEAD_SIZE, HEAD_SIZE)


def head_scores(queries, key_rows):
    return jnp.einsum(
        "rhd,sd->hrs", queries, key_rows, preferred_element_type=jnp.float32
    ) * HEAD_SIZE ** (-0.5)


def block_statistics(queries, out_grads, key_rows, value_rows):
    scores = head_scores(queries, key_rows)
    highest = jnp.max(scores, axis=2)
    weights = jnp.exp(scores - highest[:, :, None])
    products = jnp.einsum("rhd,sd->hrs", out_grads, value_rows, preferred_element_type=jnp.float32)
    return (highest, jnp.sum(weights, axis=2), jnp.sum(weights * products, axis=2))


def combine_statistics(former, latter):
    highest = jnp.maximum(former[0], latter[0])
    early_scale = jnp.exp(former[0] - highest)
    late_scale = jnp.exp(latter[0] - highest)
    return (
        highest,
        former[1] * early_scale + latter[1] * late_scale,
        former[2] * early_scale + latter[2] * late_scale,
    )


def score_grads(queries, out_grads, key_rows, value_rows, log_total, drifts):
    scores = head_scores(queries, key_rows)
    softmax_weights = jnp.exp(scores - log_total[:, :, None])
    products = jnp.einsum("rhd,sd->hrs", out_grads, value_rows, preferred_element_type=jnp.float32)
    slopes = (softmax_weights * (products - drifts[:, :, None]) * HEAD_SIZE ** (-0.5)).astype(
        jnp.bfloat16
    )
    return (softmax_weights.astype(jnp.bfloat16), slopes)


def join_heads(stacked):
    position = lax.axis_index("tp")
    part_cols = stacked.shape[2]
    bit_level = 0
    while part_cols < HEAD_SIZE:
        partner = jax.tree.map(
            lambda part, own: part.astype(own.dtype),
            partner_2(as_sent(stacked), "tp", bit_level),
            stacked,
        )
        upper_half = position >> bit_level & 1
        stacked = jnp.where(
            upper_half == 0,
            jnp.concatenate((stacked, partner), 2),
            jnp.concatenate((partner, stacked), 2),
        )
        part_cols = part_cols * 2
        bit_level = bit_level + 1
    return stacked


def split_sums(stacked, part_cols):
    position = lax.axis_index("tp")
    bit_count = (HEAD_SIZE // part_cols).bit_length() - 1
    for bit_level in reversed(range(bit_count)):
        half_cols = stacked.shape[2] // 2
        lower_half = stacked[:, :, :half_cols]
        upper_cols = stacked[:, :, half_cols:]
        upper_half = position >> bit_level & 1
        kept_half = jnp.where(upper_half == 0, lower_half, upper_cols)
        sent_half = jnp.where(upper_half == 0, upper_cols, lower_half)
        stacked = kept_half + partner_2(sent_half, "tp", bit_level)
    return stacked


def on_device(
    target,
    source,
    cotangent,
    target_gain,
    source_gain,
    query_weight,
    key_weight,
    value_projection_weight,
    output_weight,
):
    part_cols = key_weight.shape[1]
    src_scaled, src_inverse = norm_rows(source)
    src_normed = (src_scaled * source_gain).astype(jnp.bfloat16)
    tgt_scaled, tgt_inverse = norm_rows(target)
    tgt_normed = (tgt_scaled * target_gain).astype(jnp.bfloat16)
    block_rows = lax.all_gather(src_normed, "tp", axis=0, tiled=True)
    key_portion = jnp.dot(block_rows, key_weight, preferred_element_type=jnp.float32).astype(
        jnp.bfloat16
    )
    value_part = jnp.dot(
        block_rows, value_projection_weight, preferred_element_type=jnp.float32
    ).astype(jnp.bfloat16)
    parted = jnp.stack((key_portion, value_part))
    queries = split_heads(
        jnp.dot(tgt_normed, query_weight, preferred_element_type=jnp.float32).astype(jnp.bfloat16)
    )
    out_grads = split_heads(times_transposed(cotangent, output_weight).astype(jnp.bfloat16))
    head_count = queries.shape[1]
    own_rows = queries.shape[0]
    own_keys = join_heads(parted)
    all_queries, all_grads = (
        lax.all_gather(queries, "sp", axis=0, tiled=True),
        lax.all_gather(out_grads, "sp", axis=0, tiled=True),
    )
    partial_value = block_statistics(all_queries, all_grads, own_keys[0], own_keys[1])
    highest, totals, weighted = combined_all(partial_value, "sp", combine_statistics)
    log_total = highest + jnp.log(totals)
    drifts = weighted / totals
    attention, slopes = score_grads(
        all_queries, all_grads, own_keys[0], own_keys[1], log_total, drifts
    )
    key_gradient_rows = jnp.einsum(
        "hrs,rhd->sd", slopes, all_queries, preferred_element_type=jnp.float32
    )
    value_gradient_rows = jnp.einsum(
        "hrs,rhd->sd", attention, all_grads, preferred_element_type=jnp.float32
    )
    row_start = lax.axis_index("sp") * own_rows
    own_log = lax.dynamic_slice_in_dim(log_total, row_start, own_rows, 1)
    own_drifts = lax.dynamic_slice_in_dim(drifts, row_start, own_rows, 1)
    pieces = lax.all_gather(own_keys, "sp", axis=1, tiled=True)
    unused, slopes = score_grads(queries, out_grads, pieces[0], pieces[1], own_log, own_drifts)
    query_grads = jnp.einsum("hrs,sd->rhd", slopes, pieces[0], preferred_element_type=jnp.float32)
    summed = split_sums(jnp.stack((key_gradient_rows, value_gradient_rows)), part_cols)
    key_flattened = summed[0].astype(jnp.bfloat16)
    value_flattened = summed[1].astype(jnp.bfloat16)
    weight_part = lax.dot_general(
        block_rows, key_flattened, (((0,), (0,)), ((), ())), preferred_element_type=jnp.float32
    )
    key_weight_grad = lax.psum(weight_part.astype(jnp.bfloat16), "sp").astype(jnp.float32)
    source_upstream = lax.psum_scatter(
        (
            times_transposed(key_flattened, key_weight)
            + times_transposed(value_flattened, value_projection_weight)
        ).astype(jnp.bfloat16),
        "tp",
        scatter_dimension=0,
        tiled=True,
    ).astype(jnp.float32)
    source_grad = norm_back(src_scaled, src_inverse, source_gain, source_upstream)
    query_flat = query_grads.astype(jnp.bfloat16).reshape(own_rows, head_count * HEAD_SIZE)
    out_rows = own_rows // lax.axis_size("tp")
    out_start = lax.axis_index("tp") * out_rows
    target_upstream = lax.psum_scatter(
        times_transposed(query_flat, query_weight), "tp", scatter_dimension=0, tiled=True
    )
    slice_scaled = lax.dynamic_slice_in_dim(tgt_scaled, out_start, out_rows, 0)
    slice_inverse = lax.dynamic_slice_in_dim(tgt_inverse, out_start, out_rows, 0)
    slice_cotangent = lax.dynamic_slice_in_dim(cotangent, out_start, out_rows, 0)
    target_grad = slice_cotangent.astype(jnp.float32) + norm_back(
        slice_scaled, slice_inverse, target_gain, target_upstream
    )
    return (target_grad, source_grad, key_weight_grad)


def solution(mesh):
    return jax.shard_map(
        on_device,
        mesh=mesh,
        in_specs=(
            P("sp", None),
            P(("sp", "tp"), None),
            P("sp", None),
            P(),
            P(),
            P(None, "tp"),
            P(None, "tp"),
            P(None, "tp"),
            P("tp", None),
        ),
        out_specs=(P(("sp", "tp"), None), P(("sp", "tp"), None), P(None, "tp")),
        check_vma=False,
    )
```

profile of v0, /device:TPU:0, one launch (start us, length us, event | category | flops | bytes accessed | tf_op | source)
XLA Modules:
  0.0 308.4 jit_solution(17943720126214287300)
XLA Ops:
  9.5 1.7 fusion.42
  13.8 3.2 %convolution_convert_fusion.2 = bf16[128,1024]{1,0:T(8,128)(2,1)S(1)} fusion(bf16[2048,1024]{1,0:T(8,128)(2,1)} %param.16, f32[2048]{0:T(1024)} %param.14, bf16[128,2048]{1,0:T(8,128)(2,1)} %param.11, f32[128]{0:T(128)S(1)} %add_rsqrt_fusion.1, f32[128]{0:T(128)S(1)} %broadcast_multiply_fusion.5), kind=kOutput, calls=%fused_computation.38 | convolution fusion | flops 538312704 | bytes 4989952 | tf_op jit(solution)/shard_map/dot_general | solution.py:150
  18.5 3.7 %convolution_convert_fusion.1 = bf16[128,1024]{1,0:T(8,128)(2,1)S(1)} fusion(bf16[128,2048]{1,0:T(8,128)(2,1)S(1)} %copy-done.9, bf16[1024,2048]{1,0:T(8,128)(2,1)} %param.19), kind=kOutput, calls=%fused_computation.37 | convolution fusion | flops 537001984 | bytes 4980736 | tf_op jit(solution)/shard_map/dot_general | solution.py:46
  23.7 13.7 %all-gather.11.cloned.1.call-done = bf16[256,2048]{1,0:T(8,128)(2,1)} async-done(((bf16[32,2048]{1,0:T(8,128)(2,1)}), bf16[256,2048]{1,0:T(8,128)(2,1)}) %all-gather.11.cloned.1.call-update) | async-done | bytes 1048592 | tf_op jit(solution)/shard_map/all_gather | solution.py:141
  37.4 1.7 convolution_convert_fusion.4
  39.7 27.9 %all-gather.15.cloned.1.call-done = bf16[512,4,256]{2,0,1:T(8,128)(2,1)} async-done(((bf16[128,4,256]{2,0,1:T(8,128)(2,1)}), bf16[512,4,256]{2,0,1:T(8,128)(2,1)}) %all-gather.15.cloned.1.call-update) | async-done | bytes 1048592 | tf_op jit(solution)/shard_map/all_gather | solution.py:157
  67.6 1.7 bitcast_reduce_fusion
  69.3 27.8 %all-gather.17.cloned.1.call-done = bf16[512,4,256]{2,0,1:T(8,128)(2,1)} async-done(((bf16[128,4,256]{2,0,1:T(8,128)(2,1)}), bf16[512,4,256]{2,0,1:T(8,128)(2,1)}) %all-gather.17.cloned.1.call-update) | async-done | bytes 1048592 | tf_op jit(solution)/shard_map/all_gather | solution.py:158
  97.1 3.1 fusion.7
  100.2 13.1 %all-gather.5 = f32[4,4,512]{2,1,0:T(4,128)S(1)} all-gather(f32[1,4,512]{2,1,0:T(4,128)S(1)} %bitcast.163), channel_id=4, replica_groups=mesh['sp'=4,'tp'=8] {'sp'}, dimensions={0}, use_global_device_ids=true | all-gather | bytes 40960 | tf_op jit(solution)/shard_map/all_gather | solution.py:25
  113.3 13.1 %all-gather.4 = f32[4,4,512]{2,1,0:T(4,128)S(1)} all-gather(f32[1,4,512]{2,1,0:T(4,128)S(1)} %bitcast.162), channel_id=3, replica_groups=mesh['sp'=4,'tp'=8] {'sp'}, dimensions={0}, use_global_device_ids=true | all-gather | bytes 40960 | tf_op jit(solution)/shard_map/all_gather | solution.py:25
  126.5 13.1 %all-gather.3 = f32[4,4,512]{2,1,0:T(4,128)S(1)} all-gather(f32[1,4,512]{2,1,0:T(4,128)S(1)} %bitcast.161), channel_id=2, replica_groups=mesh['sp'=4,'tp'=8] {'sp'}, dimensions={0}, use_global_device_ids=true | all-gather | bytes 40960 | tf_op jit(solution)/shard_map/all_gather | solution.py:25
  140.7 2.5 fusion.20
  144.8 1.8 fusion.55
  146.6 4.6 %fusion.3 = bf16[256,2048]{1,0:T(8,128)(2,1)} fusion(f32[256,2048]{1,0:T(8,128)} %fusion.55, bf16[2048,256]{1,0:T(8,128)(2,1)} %param.18, bf16[512,4,256]{2,0,1:T(8,128)(2,1)} %all-gather.17.cloned.1.call-done, f32[256,512,4]{1,0,2:T(8,128)S(1)} %get-tuple-element.70, f32[4,512]{1,0:T(4,128)S(1)} %get-tuple-element.67), kind=kOutput, calls=%fused_computation.9 | convolution fusion | flops 539033600 | bytes 7348224 | tf_op jit(solution)/shard_map/dot_general | solution.py:46
  151.3 16.6 %all-gather.13.cloned.1.call-done = bf16[2,1024,256]{2,1,0:T(8,128)(2,1)} async-done(((bf16[2,256,256]{2,1,0:T(8,128)(2,1)}), bf16[2,1024,256]{2,1,0:T(8,128)(2,1)}) %all-gather.13.cloned.1.call-update) | async-done | bytes 1048592 | tf_op jit(solution)/shard_map/all_gather | solution.py:176
  169.5 2.9 fusion.19
  172.4 4.8 %fusion.54 = f32[128,2048]{1,0:T(8,128)} fusion(bf16[128,1024]{0,1:T(8,128)(2,1)} %bitcast.160, bf16[2048,1024]{1,0:T(8,128)(2,1)} %param.16), kind=kOutput, calls=%fused_computation.98 | convolution fusion | flops 536870912 | bytes 5505024 | tf_op jit(solution)/shard_map/dot_general | solution.py:46
  177.7 43.8 %all-reduce.2.cloned.1.call-done = bf16[2048,256]{1,0:T(8,128)(2,1)} async-done(((bf16[2048,256]{1,0:T(8,128)(2,1)}), bf16[2048,256]{1,0:T(8,128)(2,1)}) %all-reduce.2.cloned.1.call-update) | async-done | bytes 1048592 | tf_op jit(solution)/shard_map/psum | solution.py:185
  221.4 2.7 convert_element_type.79
  224.1 35.6 %reduce-scatter.5.cloned.1.call-done = bf16[32,2048]{1,0:T(8,128)(2,1)} async-done(((bf16[256,2048]{1,0:T(8,128)(2,1)}), bf16[32,2048]{1,0:T(8,128)(2,1)}) %reduce-scatter.5.cloned.1.call-update) | async-done | bytes 131088 | tf_op jit(solution)/shard_map/reduce_scatter | solution.py:186
  260.9 1.7 fusion.45
  262.6 36.3 %reduce-scatter.3.cloned.1.call-done = f32[16,2048]{1,0:T(8,128)} async-done(((f32[128,2048]{1,0:T(8,128)}), f32[16,2048]{1,0:T(8,128)}) %reduce-scatter.3.cloned.1.call-update) | async-done | bytes 131088 | tf_op jit(solution)/shard_map/reduce_scatter | solution.py:199
  299.9 1.7 multiply_add_fusion
  (77 shorter events, 15.3 us)
Async XLA Ops:
  7.2 30.3 %copy-start = (bf16[2048,256]{1,0:T(8,128)(2,1)S(1)}, bf16[2048,256]{1,0:T(8,128)(2,1)}, u32[]{:S(2)}) copy-start(bf16[2048,256]{1,0:T(8,128)(2,1)} %param.17) | copy-start | bytes 3145732
  7.2 30.2 %all-gather.11.cloned.1.call-start = ((), (), s32[]{:S(2)}) async-start(), calls=%async_computation.2 | async-start | bytes 1179648 | tf_op jit(solution)/shard_map/all_gather | solution.py:141
  11.2 56.4 %all-gather.15.cloned.1.call-start = ((), (), s32[]{:S(2)}) async-start(), calls=%async_computation.4 | async-start | bytes 1310720 | tf_op jit(solution)/shard_map/all_gather | solution.py:157
  13.8 4.7 %copy-start.9 = (bf16[128,2048]{1,0:T(8,128)(2,1)S(1)}, bf16[128,2048]{1,0:T(8,128)(2,1)}, u32[]{:S(2)}) copy-start(bf16[128,2048]{1,0:T(8,128)(2,1)} %param.13) | copy-start | bytes 1572868
  17.0 0.7 copy-start.8
  18.4 78.7 %all-gather.17.cloned.1.call-start = ((), (), s32[]{:S(2)}) async-start(), calls=%async_computation.5 | async-start | bytes 1310720 | tf_op jit(solution)/shard_map/all_gather | solution.py:158
  22.2 0.7 copy-start.6
  22.2 17.0 %copy-start.4 = (bf16[2048,256]{1,0:T(8,128)(2,1)S(1)}, bf16[2048,256]{1,0:T(8,128)(2,1)}, u32[]{:S(2)}) copy-start(bf16[2048,256]{1,0:T(8,128)(2,1)} %param.18) | copy-start | bytes 3145732
  23.7 144.2 %all-gather.13.cloned.1.call-start = ((), (), s32[]{:S(2)}) async-start(), calls=%async_computation.3 | async-start | bytes 1310720 | tf_op jit(solution)/shard_map/all_gather | solution.py:176
  37.4 1.8 copy-start.1
  140.4 81.1 %all-reduce.2.cloned.1.call-start = ((), (), s32[]{:S(2)}) async-start(), calls=%async_computation.8 | async-start | bytes 2097152 | tf_op jit(solution)/shard_map/psum | solution.py:185
  140.7 2.6 copy-start.2
  144.8 115.0 %reduce-scatter.5.cloned.1.call-start = ((), (), s32[]{:S(2)}) async-start(), calls=%async_computation.7 | async-start | bytes 1179648 | tf_op jit(solution)/shard_map/reduce_scatter | solution.py:186
  151.2 18.2 %copy-start.7 = (bf16[128,1024]{1,0:T(8,128)(2,1)S(1)}, bf16[128,1024]{1,0:T(8,128)(2,1)}, u32[]{:S(2)}) copy-start(bf16[128,1024]{1,0:T(8,128)(2,1)} %copy-done.6) | copy-start | bytes 786436
  151.2 147.6 %reduce-scatter.3.cloned.1.call-start = ((), (), s32[]{:S(2)}) async-start(), calls=%async_computation.6 | async-start | bytes 1179648 | tf_op jit(solution)/shard_map/reduce_scatter | solution.py:199
  172.4 5.0 %copy-start.3 = (bf16[128,2048]{1,0:T(8,128)(2,1)S(1)}, bf16[128,2048]{1,0:T(8,128)(2,1)}, u32[]{:S(2)}) copy-start(bf16[128,2048]{1,0:T(8,128)(2,1)} %param.11) | copy-start | bytes 1572868
  177.3 82.4 %copy-start.5 = (bf16[32,2048]{1,0:T(8,128)(2,1)S(1)}, bf16[32,2048]{1,0:T(8,128)(2,1)}, u32[]{:S(2)}) copy-start(bf16[32,2048]{1,0:T(8,128)(2,1)} %param.12) | copy-start | bytes 393220
  177.3 82.4 %copy-start.10 = (f32[2048]{0:T(1024)S(1)}, f32[2048]{0:T(1024)}, u32[]{:S(2)}) copy-start(f32[2048]{0:T(1024)} %param.15) | copy-start | bytes 24580
  177.6 121.2 %copy-start.11 = (f32[2048]{0:T(1024)S(1)}, f32[2048]{0:T(1024)}, u32[]{:S(2)}) copy-start(f32[2048]{0:T(1024)} %param.14) | copy-start | bytes 24580
Sparse Core Ops, SparseCore 0:
  11.3 26.0 all-gather.10
  39.6 27.9 all-gather.14
  69.7 27.3 all-gather.16
  140.5 27.3 all-gather.12
  170.1 51.2 all-reduce.1
  224.4 35.2 reduce-scatter.4
  262.9 35.9 reduce-scatter.2
where the time goes:
time: 309 us; the launch traced here: 308 us
  waiting for transfers between devices  202 us (65%)
  blocking collectives  39.4 us (13%)
  matrix products  33.6 us (11%)
  other arithmetic  16 us (5%)
  between operations  14.3 us (5%)
    psum x1, waiting for transfers between devices, on_device(): lax.psum(weight_part.astype(jnp.bfloat16), 'sp').astype(jnp.float32)  43.8 us
    all_gather x3, blocking collectives, combined_all(): pieces = jax.tree.map(lambda part: lax.all_gather(part, axis), value)  39.4 us
    reduce_scatter x1, waiting for transfers between devices, on_device(): lax.psum_scatter(times_transposed(query_flat, query_weight), 'tp', scatte...  36.3 us
    reduce_scatter x1, waiting for transfers between devices, on_device(): lax.psum_scatter((times_transposed(key_flattened, key_weight) + times_tra...  35.6 us
    all_gather x1, waiting for transfers between devices, on_device(): lax.all_gather(queries, 'sp', axis=0, tiled=True)  27.9 us
    all_gather x1, waiting for transfers between devices, on_device(): lax.all_gather(out_grads, 'sp', axis=0, tiled=True)  27.8 us
    all_gather x1, waiting for transfers between devices, on_device(): pieces = lax.all_gather(own_keys, 'sp', axis=1, tiled=True)  16.6 us
    dot_general x4, matrix products, times_transposed(): lax.dot_general(left, right, (((1,), (1,)), ((), ())), preferred_element_...  15 us
  transfers between devices with their start and end apart: 7, of which 7 were waited for; matrix products, arithmetic and copies ran while one was open for 13% of the time, Pallas kernels for 0%

commit v1 on v0

--- a/solution.py
+++ b/solution.py
@@ -182,7 +182,9 @@
     weight_part = lax.dot_general(
         block_rows, key_flattened, (((0,), (0,)), ((), ())), preferred_element_type=jnp.float32
     )
-    key_weight_grad = lax.psum(weight_part.astype(jnp.bfloat16), "sp").astype(jnp.float32)
+    key_weight_grad = jnp.sum(
+        lax.all_gather(weight_part.astype(jnp.bfloat16), "sp"), axis=0
+    ).astype(jnp.float32)
     source_upstream = lax.psum_scatter(
         (
             times_transposed(key_flattened, key_weight)

time: 309 us -> 341 us (1.10)
  waiting for transfers between devices: 202 us -> 230 us
    all_gather x0 -> x1, waiting for transfers between devices: none -> 79.6 us  [on_device(): lax.all_gather(weight_part.astype(jnp.bfloat16), 'sp')]
    psum x1 -> x0, waiting for transfers between devices: 43.8 us -> none  [on_device(): lax.psum(weight_part.astype(jnp.bfloat16), 'sp').astype(jnp.float32)]
    reduce_scatter x1, waiting for transfers between devices: 35.6 us -> 26.9 us  [on_device(): lax.psum_scatter((times_transposed(key_flattened, key_weight) + times_tra...]
    reduce_sum x0 -> x1, other arithmetic: none -> 3.46 us  [on_device(): jnp.sum(lax.all_gather(weight_part.astype(jnp.bfloat16), 'sp'), axis=0)]
  transfers between devices with their start and end apart: 7 -> 7, of which waited for: 7 -> 7; matrix products, arithmetic and copies ran while one was open for 13% -> 12% of each run, Pallas kernels for 0% -> 0%
where the time goes in v1:
time: 341 us
  waiting for transfers between devices  230 us (67%)
  blocking collectives  39.4 us (12%)
  matrix products  33.5 us (10%)
  other arithmetic  18.2 us (5%)
  between operations  14.4 us (4%)
  local copies, waits for them, and re-layouts  4.21 us (1%)
    all_gather x1, waiting for transfers between devices, on_device(): lax.all_gather(weight_part.astype(jnp.bfloat16), 'sp')  79.6 us
    all_gather x3, blocking collectives, combined_all(): pieces = jax.tree.map(lambda part: lax.all_gather(part, axis), value)  39.4 us
    reduce_scatter x1, waiting for transfers between devices, on_device(): lax.psum_scatter(times_transposed(query_flat, query_weight), 'tp', scatte...  36.7 us
    all_gather x1, waiting for transfers between devices, on_device(): lax.all_gather(queries, 'sp', axis=0, tiled=True)  27.9 us
    all_gather x1, waiting for transfers between devices, on_device(): lax.all_gather(out_grads, 'sp', axis=0, tiled=True)  27.8 us
    reduce_scatter x1, waiting for transfers between devices, on_device(): lax.psum_scatter((times_transposed(key_flattened, key_weight) + times_tra...  26.9 us
    all_gather x1, waiting for transfers between devices, on_device(): pieces = lax.all_gather(own_keys, 'sp', axis=1, tiled=True)  17.7 us
    dot_general x4, matrix products, times_transposed(): lax.dot_general(left, right, (((1,), (1,)), ((), ())), preferred_element_...  14.9 us
  transfers between devices with their start and end apart: 7, of which 7 were waited for; matrix products, arithmetic and copies ran while one was open for 12% of the time, Pallas kernels for 0%

profile of v1, /device:TPU:0, one launch (start us, length us, event | category | flops | bytes accessed | tf_op | source)
XLA Modules:
  0.0 340.7 jit_solution(16727794199975233364)
XLA Ops:
  10.1 1.7 fusion.42
  14.4 3.2 convolution_convert_fusion.2
  19.1 3.7 %convolution_convert_fusion.1 = bf16[128,1024]{1,0:T(8,128)(2,1)S(1)} fusion(bf16[128,2048]{1,0:T(8,128)(2,1)S(1)} %copy-done.9, bf16[1024,2048]{1,0:T(8,128)(2,1)} %param.19), kind=kOutput, calls=%fused_computation.37 | convolution fusion | flops 537001984 | bytes 4980736 | tf_op jit(solution)/shard_map/dot_general | solution.py:46
  24.4 13.7 %all-gather.13.cloned.1.call-done = bf16[256,2048]{1,0:T(8,128)(2,1)} async-done(((bf16[32,2048]{1,0:T(8,128)(2,1)}), bf16[256,2048]{1,0:T(8,128)(2,1)}) %all-gather.13.cloned.1.call-update) | async-done | bytes 1048592 | tf_op jit(solution)/shard_map/all_gather | solution.py:141
  38.0 1.7 convolution_convert_fusion.4
  40.3 27.9 %all-gather.17.cloned.1.call-done = bf16[512,4,256]{2,0,1:T(8,128)(2,1)} async-done(((bf16[128,4,256]{2,0,1:T(8,128)(2,1)}), bf16[512,4,256]{2,0,1:T(8,128)(2,1)}) %all-gather.17.cloned.1.call-update) | async-done | bytes 1048592 | tf_op jit(solution)/shard_map/all_gather | solution.py:157
  68.2 1.7 bitcast_reduce_fusion
  69.9 27.8 %all-gather.19.cloned.1.call-done = bf16[512,4,256]{2,0,1:T(8,128)(2,1)} async-done(((bf16[128,4,256]{2,0,1:T(8,128)(2,1)}), bf16[512,4,256]{2,0,1:T(8,128)(2,1)}) %all-gather.19.cloned.1.call-update) | async-done | bytes 1048592 | tf_op jit(solution)/shard_map/all_gather | solution.py:158
  97.7 3.1 fusion.7
  100.8 13.1 %all-gather.6 = f32[4,4,512]{2,1,0:T(4,128)S(1)} all-gather(f32[1,4,512]{2,1,0:T(4,128)S(1)} %bitcast.165), channel_id=4, replica_groups=mesh['sp'=4,'tp'=8] {'sp'}, dimensions={0}, use_global_device_ids=true | all-gather | bytes 40960 | tf_op jit(solution)/shard_map/all_gather | solution.py:25
  113.9 13.1 %all-gather.5 = f32[4,4,512]{2,1,0:T(4,128)S(1)} all-gather(f32[1,4,512]{2,1,0:T(4,128)S(1)} %bitcast.164), channel_id=3, replica_groups=mesh['sp'=4,'tp'=8] {'sp'}, dimensions={0}, use_global_device_ids=true | all-gather | bytes 40960 | tf_op jit(solution)/shard_map/all_gather | solution.py:25
  127.1 13.1 %all-gather.4 = f32[4,4,512]{2,1,0:T(4,128)S(1)} all-gather(f32[1,4,512]{2,1,0:T(4,128)S(1)} %bitcast.163), channel_id=2, replica_groups=mesh['sp'=4,'tp'=8] {'sp'}, dimensions={0}, use_global_device_ids=true | all-gather | bytes 40960 | tf_op jit(solution)/shard_map/all_gather | solution.py:25
  141.3 2.5 fusion.20
  143.8 1.8 fusion.55
  145.6 4.6 %fusion.3 = bf16[256,2048]{1,0:T(8,128)(2,1)} fusion(f32[256,2048]{1,0:T(8,128)} %fusion.55, bf16[2048,256]{1,0:T(8,128)(2,1)} %param.18, bf16[512,4,256]{2,0,1:T(8,128)(2,1)} %all-gather.19.cloned.1.call-done, f32[256,512,4]{1,0,2:T(8,128)S(1)} %get-tuple-element.70, f32[4,512]{1,0:T(4,128)S(1)} %get-tuple-element.67), kind=kOutput, calls=%fused_computation.9 | convolution fusion | flops 539033600 | bytes 7348224 | tf_op jit(solution)/shard_map/dot_general | solution.py:46
  150.8 17.7 %all-gather.15.cloned.1.call-done = bf16[2,1024,256]{2,1,0:T(8,128)(2,1)} async-done(((bf16[2,256,256]{2,1,0:T(8,128)(2,1)}), bf16[2,1024,256]{2,1,0:T(8,128)(2,1)}) %all-gather.15.cloned.1.call-update) | async-done | bytes 1048592 | tf_op jit(solution)/shard_map/all_gather | solution.py:176
  170.1 2.9 fusion.19
  173.0 4.9 %fusion.54 = f32[128,2048]{1,0:T(8,128)} fusion(bf16[128,1024]{0,1:T(8,128)(2,1)} %bitcast.162, bf16[2048,1024]{1,0:T(8,128)(2,1)} %param.16), kind=kOutput, calls=%fused_computation.98 | convolution fusion | flops 536870912 | bytes 5505024 | tf_op jit(solution)/shard_map/dot_general | solution.py:46
  180.1 26.9 %reduce-scatter.5.cloned.1.call-done = bf16[32,2048]{1,0:T(8,128)(2,1)} async-done(((bf16[256,2048]{1,0:T(8,128)(2,1)}), bf16[32,2048]{1,0:T(8,128)(2,1)}) %reduce-scatter.5.cloned.1.call-update) | async-done | bytes 131088 | tf_op jit(solution)/shard_map/reduce_scatter | solution.py:188
  208.1 1.7 fusion.45
  209.9 36.7 %reduce-scatter.3.cloned.1.call-done = f32[16,2048]{1,0:T(8,128)} async-done(((f32[128,2048]{1,0:T(8,128)}), f32[16,2048]{1,0:T(8,128)}) %reduce-scatter.3.cloned.1.call-update) | async-done | bytes 131088 | tf_op jit(solution)/shard_map/reduce_scatter | solution.py:201
  247.6 1.7 multiply_add_fusion
  249.3 79.6 %all-gather.21.cloned.1.call-done = bf16[8192,256]{1,0:T(8,128)(2,1)} async-done(((bf16[2048,256]{1,0:T(8,128)(2,1)}), bf16[8192,256]{1,0:T(8,128)(2,1)}) %all-gather.21.cloned.1.call-update) | async-done | bytes 4194320 | tf_op jit(solution)/shard_map/all_gather | solution.py:186
  328.9 3.5 %reduce_sum.112 = bf16[2048,256]{1,0:T(8,128)(2,1)S(1)} reduce(bf16[4,2048,256]{2,1,0:T(8,128)(2,1)} %bitcast.153, bf16[]{:T(256)} %constant.48.clone.1), dimensions={0}, to_apply=%region_15.16 | reduce | flops 1572864 | bytes 5242882 | tf_op jit(solution)/shard_map/reduce_sum | solution.py:185
  (98 shorter events, 18.2 us)
Async XLA Ops:
  7.2 30.9 %copy-start = (bf16[2048,256]{1,0:T(8,128)(2,1)S(1)}, bf16[2048,256]{1,0:T(8,128)(2,1)}, u32[]{:S(2)}) copy-start(bf16[2048,256]{1,0:T(8,128)(2,1)} %param.17) | copy-start | bytes 3145732
  7.2 30.8 %all-gather.13.cloned.1.call-start = ((), (), s32[]{:S(2)}) async-start(), calls=%async_computation.2 | async-start | bytes 1179648 | tf_op jit(solution)/shard_map/all_gather | solution.py:141
  11.8 56.4 %all-gather.17.cloned.1.call-start = ((), (), s32[]{:S(2)}) async-start(), calls=%async_computation.4 | async-start | bytes 1310720 | tf_op jit(solution)/shard_map/all_gather | solution.py:157
  13.0 4.6 %copy-start.18 = (f32[128]{0:T(128)}, f32[128]{0:T(128)S(1)}, u32[]{:S(2)}) copy-start(f32[128]{0:T(128)S(1)} %broadcast_multiply_fusion.5) | copy-start | bytes 1540
  14.4 3.2 copy-start.20
  14.4 4.7 %copy-start.9 = (bf16[128,2048]{1,0:T(8,128)(2,1)S(1)}, bf16[128,2048]{1,0:T(8,128)(2,1)}, u32[]{:S(2)}) copy-start(bf16[128,2048]{1,0:T(8,128)(2,1)} %param.13) | copy-start | bytes 1572868
  19.1 78.7 %all-gather.19.cloned.1.call-start = ((), (), s32[]{:S(2)}) async-start(), calls=%async_computation.5 | async-start | bytes 1310720 | tf_op jit(solution)/shard_map/all_gather | solution.py:158
  22.9 16.9 %copy-start.4 = (bf16[2048,256]{1,0:T(8,128)(2,1)S(1)}, bf16[2048,256]{1,0:T(8,128)(2,1)}, u32[]{:S(2)}) copy-start(bf16[2048,256]{1,0:T(8,128)(2,1)} %param.18) | copy-start | bytes 3145732
  24.3 144.2 %all-gather.15.cloned.1.call-start = ((), (), s32[]{:S(2)}) async-start(), calls=%async_computation.3 | async-start | bytes 1310720 | tf_op jit(solution)/shard_map/all_gather | solution.py:176
  141.0 66.0 %reduce-scatter.5.cloned.1.call-start = ((), (), s32[]{:S(2)}) async-start(), calls=%async_computation.7 | async-start | bytes 1179648 | tf_op jit(solution)/shard_map/reduce_scatter | solution.py:188
  150.1 19.9 %copy-start.7 = (bf16[128,1024]{1,0:T(8,128)(2,1)S(1)}, bf16[128,1024]{1,0:T(8,128)(2,1)}, u32[]{:S(2)}) copy-start(bf16[128,1024]{1,0:T(8,128)(2,1)} %copy-done.6) | copy-start | bytes 786436
  150.2 96.4 %reduce-scatter.3.cloned.1.call-start = ((), (), s32[]{:S(2)}) async-start(), calls=%async_computation.6 | async-start | bytes 1179648 | tf_op jit(solution)/shard_map/reduce_scatter | solution.py:201
  150.8 19.3 %copy-start.16 = (f32[4,128]{1,0:T(4,128)S(1)}, f32[4,128]{1,0:T(4,128)}, u32[]{:S(2)}) copy-start(f32[4,128]{1,0:T(4,128)} %get-tuple-element.72) | copy-start | bytes 6148
  150.8 19.3 %copy-start.17 = (f32[4,128]{1,0:T(4,128)S(1)}, f32[4,128]{1,0:T(4,128)}, u32[]{:S(2)}) copy-start(f32[4,128]{1,0:T(4,128)} %get-tuple-element.73) | copy-start | bytes 6148
  173.0 5.2 %copy-start.2 = (bf16[256,2048]{1,0:T(8,128)(2,1)S(1)}, bf16[256,2048]{1,0:T(8,128)(2,1)}, u32[]{:S(2)}) copy-start(bf16[256,2048]{1,0:T(8,128)(2,1)} %all-gather.13.cloned.1.call-done) | copy-start | bytes 3145732
  177.9 1.8 copy-start.21
  177.9 1.9 copy-start.3
  177.9 1.9 copy-start.19
  177.9 29.1 %copy-start.5 = (bf16[32,2048]{1,0:T(8,128)(2,1)S(1)}, bf16[32,2048]{1,0:T(8,128)(2,1)}, u32[]{:S(2)}) copy-start(bf16[32,2048]{1,0:T(8,128)(2,1)} %param.12) | copy-start | bytes 393220
  177.9 29.1 %copy-start.10 = (f32[2048]{0:T(1024)S(1)}, f32[2048]{0:T(1024)}, u32[]{:S(2)}) copy-start(f32[2048]{0:T(1024)} %param.15) | copy-start | bytes 24580
  177.9 29.1 %copy-start.13 = (f32[32]{0:T(128)S(1)}, f32[32]{0:T(128)}, u32[]{:S(2)}) copy-start(f32[32]{0:T(128)} %copy-done.12) | copy-start | bytes 388
  177.9 29.0 %copy-start.15 = (f32[32]{0:T(128)S(1)}, f32[32]{0:T(128)}, u32[]{:S(2)}) copy-start(f32[32]{0:T(128)} %copy-done.14) | copy-start | bytes 388
  177.9 151.0 %all-gather.21.cloned.1.call-start = ((), (), s32[]{:S(2)}) async-start(), calls=%async_computation.8 | async-start | bytes 5242880 | tf_op jit(solution)/shard_map/all_gather | solution.py:186
  179.7 66.9 %copy-start.11 = (f32[2048]{0:T(1024)S(1)}, f32[2048]{0:T(1024)}, u32[]{:S(2)}) copy-start(f32[2048]{0:T(1024)} %param.14) | copy-start | bytes 24580
  (5 other events, 4.9 us)
Sparse Core Ops, SparseCore 0:
  11.9 26.0 all-gather.12
  40.2 27.9 all-gather.16
  70.3 27.3 all-gather.18
  141.1 27.3 all-gather.14
  171.5 35.3 reduce-scatter.4
  210.6 35.9 reduce-scatter.2
  248.1 80.7 all-gather.20
